TPU v7x, 32 devices: a whole 2x2x4 slice. The times are simulated.
32 devices in a mesh: fs: 8 (over z, x), tp: 4 (over y, core).
Axes of the slice: x: 2, y: 2, z: 4, core: 2. Of those that a mesh axis runs over, the one named last changes fastest.
Arguments:
- normed_input: bfloat16 [16384, 2048], P('fs'), may hold values from -6 to 6
- output_cotangent: bfloat16 [16384, 2048], P('fs'), may hold values from -6 to 6
- query_grad: bfloat16 [16384, 2048], P('fs', 'tp'), may hold values from -0.75 to 0.75
- key_grad: bfloat16 [16384, 2048], P('fs', 'tp'), may hold values from -0.75 to 0.75
- attn_values: bfloat16 [16384, 2048], P('fs', 'tp'), may hold values from -0.75 to 0.75
- master_weights: float32 [3, 2048, 2048], P(None, 'fs', 'tp'), may hold values from -3 to 3
- factors: bfloat16 [3, 2048, 256], P(None, 'fs'), may hold values from -0.375 to 0.375
- moments: float32 [3, 256, 2048], P(None, 'fs', 'tp'), may hold values from -620 to 620
Outputs:
- new_weights: float32 [3, 2048, 2048], P(None, 'fs', 'tp')
- weight_copies: bfloat16 [3, 2048, 2048], P(None, None, 'tp')
- steps: float32 [3, 2048, 2048], P(None, 'fs', 'tp')
- new_moments: float32 [3, 256, 2048], P(None, 'fs', 'tp')
All inputs are finite; a program needn't handle non-finite values.
Results may differ from a plain program's by a relative error of at most 0.0055.
Values may be sent and summed in bfloat16 or wider, within the bound.
A program may use at most 128 MiB of HBM per device.

v0:
```python
import jax
import jax.numpy as jnp
from jax import lax
from jax.sharding import PartitionSpec as P


def on_device(
    normed_input,
    output_cotangent,
    query_grad,
    key_grad,
    attn_values,
    master_weights,
    factors,
    moments,
):
    rank_rows = moments.shape[1]
    width = query_grad.shape[1]
    rank = factors.shape[2]
    contract = (((0,), (0,)), ((), ()))
    whole_factors = lax.all_gather(factors, "fs", axis=1, tiled=True)
    reduced = [
        jnp.dot(normed_input, whole_factors[0], preferred_element_type=jnp.float32),
        jnp.dot(normed_input, whole_factors[1], preferred_element_type=jnp.float32),
        jnp.dot(output_cotangent, whole_factors[2], preferred_element_type=jnp.float32),
    ]
    head_sides = [query_grad, key_grad, attn_values]
    pieces = []
    for index in range(3):
        reduced_cols = reduced[index]
        pieces.append(
            lax.dot_general(
                reduced_cols,
                head_sides[index].astype(jnp.float32),
                contract,
                precision=lax.Precision.HIGHEST,
                preferred_element_type=jnp.float32,
            )
        )
    projected = lax.psum_scatter(
        jnp.concatenate(pieces, axis=1).astype(jnp.bfloat16), "fs", scatter_dimension=0, tiled=True
    ).astype(jnp.float32)
    split = projected.reshape(rank_rows, 3, width).transpose(1, 0, 2)
    new_moments = 0.8 * moments + 0.2 * split
    total = lax.psum(jnp.sum(new_moments * new_moments), ("fs", "tp"))
    entries = 3 * rank * width * lax.axis_size("tp")
    rms = jnp.sqrt(total / entries + 1e-06)
    normalized = (new_moments / rms).astype(jnp.bfloat16)
    gathered = lax.all_gather(normalized, "fs", axis=1, tiled=True)
    steps = jnp.einsum("jdr,jrc->jdc", factors, gathered, preferred_element_type=jnp.float32)
    new_weights = master_weights - 0.05 * steps
    weight_copies = lax.all_gather(new_weights.astype(jnp.bfloat16), "fs", axis=1, tiled=True)
    return (new_weights, weight_copies, steps, new_moments)


def solution(mesh):
    in_specs = (
        P("fs", None),
        P("fs", None),
        P("fs", "tp"),
        P("fs", "tp"),
        P("fs", "tp"),
        P(None, "fs", "tp"),
        P(None, "fs", None),
        P(None, "fs", "tp"),
    )
    out_specs = (P(None, "fs", "tp"), P(None, None, "tp"), P(None, "fs", "tp"), P(None, "fs", "tp"))
    return jax.shard_map(
        on_device, mesh=mesh, in_specs=in_specs, out_specs=out_specs, check_vma=False
    )
```

profile of v0, /device:TPU:0, one launch (start us, length us, event | category | flops | bytes accessed | tf_op | source)
XLA Modules:
  0.0 345.6 jit_solution(5577929369961026899)
XLA Ops:
  7.2 0.0 all-gather.3.cloned.1.call-start
  7.2 0.7 all-gather.3.cloned.1.call-update
  7.9 0.0 reduce-scatter.2.cloned.1.call-start
  8.0 65.0 %all-gather.3.cloned.1.call-done = bf16[3,2048,256]{2,1,0:T(8,128)(2,1)} async-done(((bf16[3,256,256]{2,1,0:T(8,128)(2,1)}), bf16[3,2048,256]{2,1,0:T(8,128)(2,1)}) %all-gather.3.cloned.1.call-update) | async-done | bytes 3145744 | tf_op jit(solution)/shard_map/all_gather | solution.py:21
  72.9 6.2 %fusion = f32[2048,256]{1,0:T(8,128)S(1)} fusion(bf16[2048,2048]{1,0:T(8,128)(2,1)} %param.9, bf16[3,2048,256]{2,1,0:T(8,128)(2,1)} %all-gather.3.cloned.1.call-done), kind=kOutput, calls=%fused_computation.6 | convolution fusion | flops 2147483648 | bytes 11534336 | tf_op jit(solution)/shard_map/dot_general | solution.py:25
  79.2 1.9 convolution_convert_fusion
  81.2 2.5 fusion.1
  83.7 1.8 convolution_convert_fusion.1
  85.5 2.5 fusion.2
  88.0 2.0 convolution_convert_fusion.2
  90.0 0.9 pad_maximum_fusion
  91.0 0.0 all-gather.5.cloned.1.call-start
  91.1 3.1 copy.18
  94.2 58.9 %reduce-scatter.2.cloned.1.call-done = bf16[32,1536]{1,0:T(8,128)(2,1)} async-done(((bf16[256,1536]{1,0:T(8,128)(2,1)}), bf16[32,1536]{1,0:T(8,128)(2,1)}) %reduce-scatter.2.cloned.1.call-update) | async-done | bytes 98320 | tf_op jit(solution)/shard_map/reduce_scatter | solution.py:40
  153.1 0.9 convert_multiply_fusion
  154.0 0.7 multiply_reduce_fusion
  154.7 40.0 %psum.7 = f32[]{:T(128)} all-reduce(f32[]{:T(128)} %get-tuple-element.14), channel_id=1, replica_groups=mesh['fs'=8,'tp'=4] {'fs','tp'}, use_global_device_ids=true, to_apply=%region_2.0 | all-reduce | flops 1 | bytes 8 | tf_op jit(solution)/shard_map/psum | solution.py:45
  195.4 32.0 %all_gather.10 = bf16[3,256,512]{2,1,0:T(8,128)(2,1)S(1)} all-gather(bf16[3,32,512]{2,1,0:T(8,128)(2,1)S(1)} %divide_convert_fusion), channel_id=1, replica_groups=mesh['fs'=8,'tp'=4] {'fs'}, dimensions={1}, use_global_device_ids=true | all-gather | bytes 884736 | tf_op jit(solution)/shard_map/all_gather | solution.py:49
  227.5 3.9 %fusion.4 = (bf16[3,256,512]{1,2,0:T(8,128)(2,1)}, f32[3,256,512]{1,2,0:T(8,128)}, f32[3,256,512]{1,2,0:T(8,128)}) fusion(f32[3,256,512]{1,2,0:T(8,128)} %copy.18, bf16[3,256,512]{2,1,0:T(8,128)(2,1)S(1)} %all_gather.10, bf16[3,256,256]{2,1,0:T(8,128)(2,1)S(1)} %copy-done.3), kind=kOutput, calls=%fused_computation.17 | convolution fusion | flops 202506240 | bytes 6684672 | tf_op jit(solution)/shard_map/jdr,jrc->jdc/dot_general | solution.py:50
  231.3 0.0 all-gather.5.cloned.1.call-update
  231.4 3.0 copy.19
  234.4 3.0 copy.21
  237.4 93.1 %all-gather.5.cloned.1.call-done = bf16[3,2048,512]{1,2,0:T(8,128)(2,1)} async-done(((bf16[3,256,512]{1,2,0:T(8,128)(2,1)}), bf16[3,2048,512]{1,2,0:T(8,128)(2,1)}) %all-gather.5.cloned.1.call-update) | async-done | bytes 6291472 | tf_op jit(solution)/shard_map/all_gather | solution.py:52
  330.5 8.6 %copy.20 = bf16[3,2048,512]{2,1,0:T(8,128)(2,1)} copy(bf16[3,2048,512]{1,2,0:T(8,128)(2,1)} %all-gather.5.cloned.1.call-done) | data formatting | bytes 12582912
  (18 shorter events, 0.1 us)
Async XLA Ops:
  7.2 72.0 %copy-start = (bf16[2048,512]{1,0:T(8,128)(2,1)S(1)}, bf16[2048,512]{1,0:T(8,128)(2,1)}, u32[]{:S(2)}) copy-start(bf16[2048,512]{1,0:T(8,128)(2,1)} %param.12) | copy-start | bytes 6291460
  7.2 65.8 %all-gather.3.cloned.1.call-start = ((), (), s32[]{:S(2)}) async-start(), calls=%async_computation.1 | async-start | bytes 3538944 | tf_op jit(solution)/shard_map/all_gather | solution.py:21
  7.9 145.2 %reduce-scatter.2.cloned.1.call-start = ((), (), s32[]{:S(2)}) async-start(), calls=%async_computation.2 | async-start | bytes 884736 | tf_op jit(solution)/shard_map/reduce_scatter | solution.py:40
  72.9 8.2 %copy-start.6 = (bf16[2048,2048]{1,0:T(8,128)(2,1)S(1)}, bf16[2048,2048]{1,0:T(8,128)(2,1)}, u32[]{:S(2)}) copy-start(bf16[2048,2048]{1,0:T(8,128)(2,1)} %param.8) | copy-start | bytes 25165828
  79.2 2.0 copy-start.7
  81.2 2.5 copy-start.1
  85.5 2.5 copy-start.2
  91.0 63.0 %copy-start.5 = (f32[3,32,512]{2,1,0:T(8,128)S(1)}, f32[3,32,512]{2,1,0:T(8,128)}, u32[]{:S(2)}) copy-start(f32[3,32,512]{2,1,0:T(8,128)} %param.15) | copy-start | bytes 589828
  91.0 136.5 %copy-start.3 = (bf16[3,256,256]{2,1,0:T(8,128)(2,1)S(1)}, bf16[3,256,256]{2,1,0:T(8,128)(2,1)}, u32[]{:S(2)}) copy-start(bf16[3,256,256]{2,1,0:T(8,128)(2,1)} %param.14) | copy-start | bytes 1179652
  91.0 239.5 %all-gather.5.cloned.1.call-start = ((), (), s32[]{:S(2)}) async-start(), calls=%async_computation.3 | async-start | bytes 7077888 | tf_op jit(solution)/shard_map/all_gather | solution.py:52
  154.7 76.7 %copy-start.4 = (f32[3,32,512]{2,1,0:T(8,128)}, f32[3,32,512]{2,1,0:T(8,128)S(1)}, u32[]{:S(2)}) copy-start(f32[3,32,512]{2,1,0:T(8,128)S(1)} %get-tuple-element.15) | copy-start | bytes 589828
Sparse Core Ops, SparseCore 0:
  10.2 62.7 all-gather.2
  91.1 61.9 reduce-scatter.1
  231.5 98.9 all-gather.4
where the time goes:
time: 346 us
  waiting for transfers between devices  218 us (63%)
  blocking collectives  72.1 us (21%)
  matrix products  20.8 us (6%)
  local copies, waits for them, and re-layouts  17.8 us (5%)
  between operations  14.6 us (4%)
    all_gather x1, waiting for transfers between devices, on_device(): lax.all_gather(new_weights.astype(jnp.bfloat16), 'fs', axis=1, tiled=True)  93.1 us
    all_gather x1, waiting for transfers between devices, on_device(): whole_factors = lax.all_gather(factors, 'fs', axis=1, tiled=True)  65 us
    reduce_scatter x1, waiting for transfers between devices, on_device(): lax.psum_scatter(jnp.concatenate(pieces, axis=1).astype(jnp.bfloat16), 'f...  58.9 us
    psum x1, blocking collectives, on_device(): total = lax.psum(jnp.sum(new_moments * new_moments), ('fs', 'tp'))  40 us
    all_gather x1, blocking collectives, on_device(): gathered = lax.all_gather(normalized, 'fs', axis=1, tiled=True)  32 us
    unnamed x20, local copies, waits for them, and re-layouts  17.8 us
  transfers between devices with their start and end apart: 3, of which 3 were waited for; matrix products, arithmetic and copies ran while one was open for 3% of the time, Pallas kernels for 0%

commit v1 on v0

--- a/solution.py
+++ b/solution.py
@@ -46,8 +46,22 @@
     entries = 3 * rank * width * lax.axis_size("tp")
     rms = jnp.sqrt(total / entries + 1e-06)
     normalized = (new_moments / rms).astype(jnp.bfloat16)
-    gathered = lax.all_gather(normalized, "fs", axis=1, tiled=True)
-    steps = jnp.einsum("jdr,jrc->jdc", factors, gathered, preferred_element_type=jnp.float32)
+    size, index_2, width_2 = (lax.axis_size("fs"), lax.axis_index("fs"), normalized.shape[1])
+    ahead = [(i, (i + 1) % size) for i in range(size)]
+    held, total_2 = (normalized, None)
+    for lap in range(size):
+        coming = lax.ppermute(held, "fs", ahead) if lap < size - 1 else None
+        absorb = jnp.einsum(
+            "jdr,jrc->jdc",
+            lax.dynamic_slice_in_dim(
+                factors, (index_2 - lap) % size * width_2, held.shape[1], axis=2
+            ),
+            held,
+            preferred_element_type=jnp.float32,
+        )
+        total_2 = absorb if total_2 is None else total_2 + absorb
+        held = coming
+    steps = total_2
     new_weights = master_weights - 0.05 * steps
     weight_copies = lax.all_gather(new_weights.astype(jnp.bfloat16), "fs", axis=1, tiled=True)
     return (new_weights, weight_copies, steps, new_moments)

time: 346 us -> 360 us (1.040)
  waiting for transfers between devices: 218 us -> 272 us
  blocking collectives: 72.1 us -> 40.1 us
  local copies, waits for them, and re-layouts: 17.8 us -> 5.94 us
    ppermute x0 -> x7, waiting for transfers between devices: none -> 46.9 us  [on_device(): coming = lax.ppermute(held, 'fs', ahead) if lap < size - 1 else None]
    all_gather x1 -> x0, blocking collectives: 32 us -> none  [on_device(): gathered = lax.all_gather(normalized, 'fs', axis=1, tiled=True)]
    unnamed x20 -> x19, local copies, waits for them, and re-layouts: 17.8 us -> 5.94 us
    all_gather x1, waiting for transfers between devices: 93.1 us -> 97.2 us  [on_device(): lax.all_gather(new_weights.astype(jnp.bfloat16), 'fs', axis=1, tiled=True)]
  transfers between devices with their start and end apart: 3 -> 10, of which waited for: 3 -> 10; matrix products, arithmetic and copies ran while one was open for 3% -> 1% of each run, Pallas kernels for 0% -> 0%
where the time goes in v1:
time: 360 us
  waiting for transfers between devices  272 us (76%)
  blocking collectives  40.1 us (11%)
  matrix products  22.5 us (6%)
  between operations  14.8 us (4%)
  local copies, waits for them, and re-layouts  5.94 us (2%)
    all_gather x1, waiting for transfers between devices, on_device(): lax.all_gather(new_weights.astype(jnp.bfloat16), 'fs', axis=1, tiled=True)  97.2 us
    all_gather x1, waiting for transfers between devices, on_device(): whole_factors = lax.all_gather(factors, 'fs', axis=1, tiled=True)  65 us
    reduce_scatter x1, waiting for transfers between devices, on_device(): lax.psum_scatter(jnp.concatenate(pieces, axis=1).astype(jnp.bfloat16), 'f...  61.9 us
    ppermute x7, waiting for transfers between devices, on_device(): coming = lax.ppermute(held, 'fs', ahead) if lap < size - 1 else None  46.9 us
    psum x1, blocking collectives, on_device(): total = lax.psum(jnp.sum(new_moments * new_moments), ('fs', 'tp'))  40.1 us
  transfers between devices with their start and end apart: 10, of which 10 were waited for; matrix products, arithmetic and copies ran while one was open for 1% of the time, Pallas kernels for 0%

profile of v1, /device:TPU:0, one launch (start us, length us, event | category | flops | bytes accessed | tf_op | source)
XLA Modules:
  0.0 360.0 jit_solution(11589937479913070164)
XLA Ops:
  7.2 0.7 all-gather.3.cloned.1.call-update
  8.0 65.0 %all-gather.3.cloned.1.call-done = bf16[3,2048,256]{2,1,0:T(8,128)(2,1)} async-done(((bf16[3,256,256]{2,1,0:T(8,128)(2,1)}), bf16[3,2048,256]{2,1,0:T(8,128)(2,1)}) %all-gather.3.cloned.1.call-update) | async-done | bytes 3145744 | tf_op jit(solution)/shard_map/all_gather | solution.py:21
  72.9 6.2 %fusion = f32[2048,256]{1,0:T(8,128)S(1)} fusion(bf16[2048,2048]{1,0:T(8,128)(2,1)} %param.9, bf16[3,2048,256]{2,1,0:T(8,128)(2,1)} %all-gather.3.cloned.1.call-done), kind=kOutput, calls=%fused_computation.6 | convolution fusion | flops 2147483648 | bytes 11534336 | tf_op jit(solution)/shard_map/dot_general | solution.py:25
  79.2 1.9 convolution_convert_fusion
  81.2 2.5 fusion.1
  83.7 1.8 convolution_convert_fusion.1
  85.5 2.5 fusion.2
  88.0 2.0 convolution_convert_fusion.2
  90.1 0.9 pad_maximum_fusion
  91.2 61.9 %reduce-scatter.2.cloned.1.call-done = bf16[32,1536]{1,0:T(8,128)(2,1)} async-done(((bf16[256,1536]{1,0:T(8,128)(2,1)}), bf16[32,1536]{1,0:T(8,128)(2,1)}) %reduce-scatter.2.cloned.1.call-update) | async-done | bytes 98320 | tf_op jit(solution)/shard_map/reduce_scatter | solution.py:40
  153.1 0.9 convert_multiply_fusion
  154.0 0.7 multiply_reduce_fusion
  154.7 40.1 %psum.7 = f32[]{:T(128)} all-reduce(f32[]{:T(128)} %get-tuple-element.6), channel_id=1, replica_groups=mesh['fs'=8,'tp'=4] {'fs','tp'}, use_global_device_ids=true, to_apply=%region_2.0 | all-reduce | flops 1 | bytes 8 | tf_op jit(solution)/shard_map/psum | solution.py:45
  195.5 2.3 collective-permute-start
  198.2 4.6 %collective-permute-done = bf16[3,32,512]{2,1,0:T(8,128)(2,1)S(1)} collective-permute-done((bf16[3,32,512]{2,1,0:T(8,128)(2,1)S(1)}, bf16[3,32,512]{2,1,0:T(8,128)(2,1)S(1)}, u32[]{:S(2)}, u32[]{:S(2)}) %collective-permute-start) | collective-permute-done | bytes 98336 | tf_op jit(solution)/shard_map/ppermute | solution.py:53
  203.3 6.9 %collective-permute-done.1 = bf16[3,32,512]{2,1,0:T(8,128)(2,1)S(1)} collective-permute-done((bf16[3,32,512]{2,1,0:T(8,128)(2,1)S(1)}, bf16[3,32,512]{2,1,0:T(8,128)(2,1)S(1)}, u32[]{:S(2)}, u32[]{:S(2)}) %collective-permute-start.1) | collective-permute-done | bytes 98336 | tf_op jit(solution)/shard_map/ppermute | solution.py:53
  210.6 6.9 %collective-permute-done.2 = bf16[3,32,512]{2,1,0:T(8,128)(2,1)S(1)} collective-permute-done((bf16[3,32,512]{2,1,0:T(8,128)(2,1)S(1)}, bf16[3,32,512]{2,1,0:T(8,128)(2,1)S(1)}, u32[]{:S(2)}, u32[]{:S(2)}) %collective-permute-start.2) | collective-permute-done | bytes 98336 | tf_op jit(solution)/shard_map/ppermute | solution.py:53
  217.9 7.0 %collective-permute-done.3 = bf16[3,32,512]{2,1,0:T(8,128)(2,1)S(1)} collective-permute-done((bf16[3,32,512]{2,1,0:T(8,128)(2,1)S(1)}, bf16[3,32,512]{2,1,0:T(8,128)(2,1)S(1)}, u32[]{:S(2)}, u32[]{:S(2)}) %collective-permute-start.3) | collective-permute-done | bytes 98336 | tf_op jit(solution)/shard_map/ppermute | solution.py:53
  225.3 7.7 %collective-permute-done.4 = bf16[3,32,512]{2,1,0:T(8,128)(2,1)S(1)} collective-permute-done((bf16[3,32,512]{2,1,0:T(8,128)(2,1)S(1)}, bf16[3,32,512]{2,1,0:T(8,128)(2,1)S(1)}, u32[]{:S(2)}, u32[]{:S(2)}) %collective-permute-start.4) | collective-permute-done | bytes 98336 | tf_op jit(solution)/shard_map/ppermute | solution.py:53
  233.5 6.9 %collective-permute-done.5 = bf16[3,32,512]{2,1,0:T(8,128)(2,1)S(1)} collective-permute-done((bf16[3,32,512]{2,1,0:T(8,128)(2,1)S(1)}, bf16[3,32,512]{2,1,0:T(8,128)(2,1)S(1)}, u32[]{:S(2)}, u32[]{:S(2)}) %collective-permute-start.5) | collective-permute-done | bytes 98336 | tf_op jit(solution)/shard_map/ppermute | solution.py:53
  240.8 6.9 %collective-permute-done.6 = bf16[3,32,512]{2,1,0:T(8,128)(2,1)S(1)} collective-permute-done((bf16[3,32,512]{2,1,0:T(8,128)(2,1)S(1)}, bf16[3,32,512]{2,1,0:T(8,128)(2,1)S(1)}, u32[]{:S(2)}, u32[]{:S(2)}) %collective-permute-start.6) | collective-permute-done | bytes 98336 | tf_op jit(solution)/shard_map/ppermute | solution.py:53
  247.7 2.7 fusion.27
  250.4 97.2 %all-gather.5.cloned.1.call-done = bf16[3,2048,512]{2,1,0:T(8,128)(2,1)} async-done(((bf16[3,256,512]{2,1,0:T(8,128)(2,1)}), bf16[3,2048,512]{2,1,0:T(8,128)(2,1)}) %all-gather.5.cloned.1.call-update) | async-done | bytes 6291472 | tf_op jit(solution)/shard_map/all_gather | solution.py:66
  347.6 5.9 %copy.42 = bf16[3,2048,512]{2,1,0:T(8,128)(2,1)} copy(bf16[3,2048,512]{2,1,0:T(8,128)(2,1)} %all-gather.5.cloned.1.call-done) | data formatting | bytes 12582912
  (37 shorter events, 3.1 us)
Async XLA Ops:
  7.2 72.0 %copy-start = (bf16[2048,512]{1,0:T(8,128)(2,1)S(1)}, bf16[2048,512]{1,0:T(8,128)(2,1)}, u32[]{:S(2)}) copy-start(bf16[2048,512]{1,0:T(8,128)(2,1)} %param.12) | copy-start | bytes 6291460
  7.2 65.8 %all-gather.3.cloned.1.call-start = ((), (), s32[]{:S(2)}) async-start(), calls=%async_computation.1 | async-start | bytes 3538944 | tf_op jit(solution)/shard_map/all_gather | solution.py:21
  7.9 145.2 %reduce-scatter.2.cloned.1.call-start = ((), (), s32[]{:S(2)}) async-start(), calls=%async_computation.2 | async-start | bytes 884736 | tf_op jit(solution)/shard_map/reduce_scatter | solution.py:40
  72.9 8.2 %copy-start.7 = (bf16[2048,2048]{1,0:T(8,128)(2,1)S(1)}, bf16[2048,2048]{1,0:T(8,128)(2,1)}, u32[]{:S(2)}) copy-start(bf16[2048,2048]{1,0:T(8,128)(2,1)} %param.8) | copy-start | bytes 25165828
  79.2 2.0 copy-start.8
  81.2 2.5 copy-start.2
  85.5 2.5 copy-start.3
  90.0 64.0 %copy-start.6 = (f32[3,32,512]{2,1,0:T(8,128)S(1)}, f32[3,32,512]{2,1,0:T(8,128)}, u32[]{:S(2)}) copy-start(f32[3,32,512]{2,1,0:T(8,128)} %param.15) | copy-start | bytes 589828
  90.1 107.8 %copy-start.1 = (bf16[3,256,256]{2,1,0:T(8,128)(2,1)S(1)}, bf16[3,256,256]{2,1,0:T(8,128)(2,1)}, u32[]{:S(2)}) copy-start(bf16[3,256,256]{2,1,0:T(8,128)(2,1)} %param.14) | copy-start | bytes 1179652
  91.0 256.6 %all-gather.5.cloned.1.call-start = ((), (), s32[]{:S(2)}) async-start(), calls=%async_computation.3 | async-start | bytes 7077888 | tf_op jit(solution)/shard_map/all_gather | solution.py:66
  154.7 55.9 %copy-start.5 = (f32[3,32,512]{2,1,0:T(8,128)}, f32[3,32,512]{2,1,0:T(8,128)S(1)}, u32[]{:S(2)}) copy-start(f32[3,32,512]{2,1,0:T(8,128)S(1)} %get-tuple-element.16) | copy-start | bytes 589828
  195.5 7.4 %collective-permute-start = (bf16[3,32,512]{2,1,0:T(8,128)(2,1)S(1)}, bf16[3,32,512]{2,1,0:T(8,128)(2,1)S(1)}, u32[]{:S(2)}, u32[]{:S(2)}) collective-permute-start(bf16[3,32,512]{2,1,0:T(8,128)(2,1)S(1)} %divide_convert_fusion), channel_id=1, source_target_pairs={{0,4},{4,8},{8,12},{12,16},{16,20},{20,24},{24,28},{28,0},{1,5},{5... | collective-permute-start | bytes 294920 | tf_op jit(solution)/shard_map/ppermute | solution.py:53
  202.9 7.3 %collective-permute-start.1 = (bf16[3,32,512]{2,1,0:T(8,128)(2,1)S(1)}, bf16[3,32,512]{2,1,0:T(8,128)(2,1)S(1)}, u32[]{:S(2)}, u32[]{:S(2)}) collective-permute-start(bf16[3,32,512]{2,1,0:T(8,128)(2,1)S(1)} %collective-permute-done), channel_id=1, source_target_pairs={{0,4},{4,8},{8,12},{12,16},{16,20},{20,24},{24,28},{28,0},{1,5},{5... | collective-permute-start | bytes 294920 | tf_op jit(solution)/shard_map/ppermute | solution.py:53
  210.2 7.3 %collective-permute-start.2 = (bf16[3,32,512]{2,1,0:T(8,128)(2,1)S(1)}, bf16[3,32,512]{2,1,0:T(8,128)(2,1)S(1)}, u32[]{:S(2)}, u32[]{:S(2)}) collective-permute-start(bf16[3,32,512]{2,1,0:T(8,128)(2,1)S(1)} %collective-permute-done.1), channel_id=1, source_target_pairs={{0,4},{4,8},{8,12},{12,16},{16,20},{20,24},{24,28},{28,0},{1,5},{5... | collective-permute-start | bytes 294920 | tf_op jit(solution)/shard_map/ppermute | solution.py:53
  217.5 7.4 %collective-permute-start.3 = (bf16[3,32,512]{2,1,0:T(8,128)(2,1)S(1)}, bf16[3,32,512]{2,1,0:T(8,128)(2,1)S(1)}, u32[]{:S(2)}, u32[]{:S(2)}) collective-permute-start(bf16[3,32,512]{2,1,0:T(8,128)(2,1)S(1)} %collective-permute-done.2), channel_id=1, source_target_pairs={{0,4},{4,8},{8,12},{12,16},{16,20},{20,24},{24,28},{28,0},{1,5},{5... | collective-permute-start | bytes 294920 | tf_op jit(solution)/shard_map/ppermute | solution.py:53
  224.9 8.2 %collective-permute-start.4 = (bf16[3,32,512]{2,1,0:T(8,128)(2,1)S(1)}, bf16[3,32,512]{2,1,0:T(8,128)(2,1)S(1)}, u32[]{:S(2)}, u32[]{:S(2)}) collective-permute-start(bf16[3,32,512]{2,1,0:T(8,128)(2,1)S(1)} %collective-permute-done.3), channel_id=1, source_target_pairs={{0,4},{4,8},{8,12},{12,16},{16,20},{20,24},{24,28},{28,0},{1,5},{5... | collective-permute-start | bytes 294920 | tf_op jit(solution)/shard_map/ppermute | solution.py:53
  225.3 22.4 %copy-start.4 = (f32[3,256,512]{2,1,0:T(8,128)S(1)}, f32[3,256,512]{2,1,0:T(8,128)}, u32[]{:S(2)}) copy-start(f32[3,256,512]{2,1,0:T(8,128)} %param.13) | copy-start | bytes 4718596
  233.1 7.3 %collective-permute-start.5 = (bf16[3,32,512]{2,1,0:T(8,128)(2,1)S(1)}, bf16[3,32,512]{2,1,0:T(8,128)(2,1)S(1)}, u32[]{:S(2)}, u32[]{:S(2)}) collective-permute-start(bf16[3,32,512]{2,1,0:T(8,128)(2,1)S(1)} %collective-permute-done.4), channel_id=1, source_target_pairs={{0,4},{4,8},{8,12},{12,16},{16,20},{20,24},{24,28},{28,0},{1,5},{5... | collective-permute-start | bytes 294920 | tf_op jit(solution)/shard_map/ppermute | solution.py:53
  240.4 7.3 %collective-permute-start.6 = (bf16[3,32,512]{2,1,0:T(8,128)(2,1)S(1)}, bf16[3,32,512]{2,1,0:T(8,128)(2,1)S(1)}, u32[]{:S(2)}, u32[]{:S(2)}) collective-permute-start(bf16[3,32,512]{2,1,0:T(8,128)(2,1)S(1)} %collective-permute-done.5), channel_id=1, source_target_pairs={{0,4},{4,8},{8,12},{12,16},{16,20},{20,24},{24,28},{28,0},{1,5},{5... | collective-permute-start | bytes 294920 | tf_op jit(solution)/shard_map/ppermute | solution.py:53
Sparse Core Ops, SparseCore 0:
  10.2 62.7 all-gather.2
  91.1 61.9 reduce-scatter.1
  250.6 97.0 all-gather.4
